TPU v7x, 32 devices: a whole 2x2x4 slice. The times are simulated.
32 devices in a mesh: ep: 8 (over z, core), tp: 4 (over y, x).
Axes of the slice: x: 2, y: 2, z: 4, core: 2. Of those that a mesh axis runs over, the one named last changes fastest.
Arguments:
- queries: bfloat16 [2048, 2048], P('ep', 'tp'), may hold values from -6 to 6
- keys: bfloat16 [2048, 2048], P('ep', 'tp'), may hold values from -6 to 6
- values: bfloat16 [2048, 2048], P('ep', 'tp'), may hold values from -6 to 6
- gates: bfloat16 [2048, 2048], P('ep', 'tp'), may hold values from -6 to 6
- log_decay: float32 [2048, 16], P('ep', 'tp'), may hold values from -2 to 0
- out_weight: bfloat16 [2048, 2048], P(None, 'tp'), may hold values from -0.125 to 0.125
- moe_rows: bfloat16 [2048, 2048], P('ep'), may hold values from -140 to 140
- moe_gain: bfloat16 [2048], replicated, may hold values from 0.099609375 to 1.8984375
- routes: int32 [2048, 2], P('ep'), may hold values from 0 to 7, as said below
- route_weights: float32 [2048, 2], P('ep'), may hold values from 0.1 to 1
- gate_proj: bfloat16 [8, 2048, 4096], P('ep', None, 'tp'), may hold values from -0.125 to 0.125
- up_proj: bfloat16 [8, 2048, 4096], P('ep', None, 'tp'), may hold values from -0.125 to 0.125
- down_proj: bfloat16 [8, 4096, 2048], P('ep', None, 'tp'), may hold values from -0.09375 to 0.09375
Outputs:
- mixer_out: bfloat16 [2048, 2048], P('ep', 'tp')
- moe_out: bfloat16 [2048, 2048], P('ep', 'tp')
Inputs may be any that keep to these rules, and one draw needn't show every extreme that they name: `routes`: each row names two different experts of one group of 8 consecutive experts; in each aligned block of 256 rows every expert is named by exactly 64 rows.
All inputs are finite; a program needn't handle non-finite values.
Results may differ from a plain program's by a relative error of at most 0.011.
Values may be sent and summed in bfloat16 or wider, within the bound.
A program may use at most 64 MiB of HBM per device.

v0:
```python
import jax
import jax.numpy as jnp
from jax import lax
from jax.sharding import PartitionSpec as P

BLOCK = 128


def carried_in(value, axis, join, neutral):
    count, mine = (lax.axis_size(axis), lax.axis_index(axis))
    pieces = jax.tree.map(lambda part: lax.all_gather(part, axis), value)
    total = jax.tree.map(
        lambda part, zero: jnp.full_like(part, 0) + jnp.asarray(zero, part.dtype), value, neutral
    )

    def turn(position, total):
        longer = join(total, jax.tree.map(lambda part: part[position], pieces))
        return jax.tree.map(lambda new, old: jnp.where(position < mine, new, old), longer, total)

    return lax.fori_loop(0, count - 1, turn, total)


def rotate(source, positions, heads_here, factor):
    row_count, feat_width = source.shape
    head_dim = feat_width // heads_here
    half_dim = head_dim // 2
    values_f = source.astype(jnp.float32).reshape(row_count, heads_here, head_dim)
    inverse = 10000.0 ** (-jnp.arange(half_dim, dtype=jnp.float32) / half_dim)
    angles = positions[:, None] * inverse[None, :]
    cosine = jnp.cos(angles)[:, None, :]
    sine_part = jnp.sin(angles)[:, None, :]
    first_half = values_f[..., :half_dim]
    second_half = values_f[..., half_dim:]
    turned = jnp.concatenate(
        [
            first_half * cosine - second_half * sine_part,
            first_half * sine_part + second_half * cosine,
        ],
        axis=-1,
    )
    return (turned * factor).astype(jnp.bfloat16).reshape(row_count, feat_width)


def chain_states(earlier, later):
    return (earlier[0] * later[0], later[0][:, None, None] * earlier[1] + later[1])


def retention_half(queries, keys, values, gates, log_decay, out_weight):
    row_count, feat_width = queries.shape
    heads_here = log_decay.shape[1]
    head_dim = feat_width // heads_here
    block_count = row_count // BLOCK
    positions = (lax.axis_index("ep") * row_count + jnp.arange(row_count, dtype=jnp.int32)).astype(
        jnp.float32
    )
    rot_q = rotate(queries, positions, heads_here, 1.0)
    rot_k = rotate(keys, positions, heads_here, head_dim ** (-0.5))
    block_shape = (block_count, BLOCK, heads_here, head_dim)
    q_blocks = rot_q.reshape(block_shape)
    k_blocks = rot_k.reshape(block_shape)
    v_blocks = values.reshape(block_shape)
    cumulative = jnp.cumsum(log_decay.reshape(block_count, BLOCK, heads_here), axis=1)
    across = jnp.swapaxes(cumulative, 1, 2)
    spread = across[..., :, None] - across[..., None, :]
    causal = jnp.arange(BLOCK)[:, None] >= jnp.arange(BLOCK)[None, :]
    weights = jnp.where(causal, jnp.exp(jnp.where(causal, spread, 0.0)), 0.0)
    scores = jnp.einsum("nihd,njhd->nhij", q_blocks, k_blocks, preferred_element_type=jnp.float32)
    rounded = (scores * weights).astype(jnp.bfloat16)
    inside = jnp.einsum("nhij,njhd->nihd", rounded, v_blocks, preferred_element_type=jnp.float32)
    ending = cumulative[:, -1, :]
    k_scaled = k_blocks.astype(jnp.float32) * jnp.exp(ending[:, None, :] - cumulative)[..., None]
    updates = jnp.einsum(
        "njhd,njhe->nhde", k_scaled, v_blocks.astype(jnp.float32), precision=lax.Precision.HIGHEST
    )

    def advance(carry_state, member):
        return (jnp.exp(member[0])[:, None, None] * carry_state + member[1], carry_state)

    zero_state = jnp.zeros((heads_here, head_dim, head_dim), jnp.float32)
    local_end, before = lax.scan(advance, zero_state, (ending, updates))
    device_decay = jnp.exp(jnp.sum(ending, axis=0))
    incoming = carried_in(
        (device_decay, local_end), "ep", chain_states, (jnp.ones_like(device_decay), zero_state)
    )
    leading = jnp.cumsum(ending, axis=0) - ending
    entering = before + jnp.exp(leading)[:, :, None, None] * incoming[1][None]
    carried = (
        jnp.einsum(
            "nihd,nhde->nihe",
            q_blocks.astype(jnp.float32),
            entering,
            precision=lax.Precision.HIGHEST,
        )
        * jnp.exp(cumulative)[..., None]
    )
    retained = (inside + carried).reshape(row_count, heads_here, head_dim)
    gate_f = gates.astype(jnp.float32).reshape(row_count, heads_here, head_dim)
    scaled = retained * lax.rsqrt(jnp.mean(retained * retained, axis=-1, keepdims=True) + 1e-05)
    head_out = (scaled * jax.nn.silu(gate_f)).astype(jnp.bfloat16).reshape(row_count, feat_width)
    projected = jnp.dot(
        lax.all_gather(head_out, "tp", axis=1, tiled=True),
        out_weight,
        preferred_element_type=jnp.float32,
    )
    return projected.astype(jnp.bfloat16)


def expert_half(moe_rows, moe_gain, routes, route_weights, gate_proj, up_proj, down_proj):
    row_count, feat_width = moe_rows.shape
    experts = lax.axis_size("ep")
    capacity = 2 * row_count // experts
    as_float = moe_rows.astype(jnp.float32)
    normed = (
        as_float
        * lax.rsqrt(jnp.mean(as_float * as_float, axis=-1, keepdims=True) + 1e-06)
        * moe_gain.astype(jnp.float32)
    ).astype(jnp.bfloat16)
    flat_ids = routes.reshape(-1)
    onehot = (flat_ids[:, None] == jnp.arange(experts, dtype=jnp.int32)[None, :]).astype(jnp.int32)
    slot_rank = jnp.sum((jnp.cumsum(onehot, axis=0) - onehot) * onehot, axis=1)
    target = flat_ids * capacity + slot_rank
    source_row = (
        jnp.zeros((experts * capacity,), jnp.int32)
        .at[target]
        .set(jnp.arange(2 * row_count, dtype=jnp.int32) // 2)
    )
    outgoing = normed[source_row].reshape(experts, capacity, feat_width)
    w_gate = gate_proj[0]
    w_up = up_proj[0]
    w_down = down_proj[0]
    arrived_rows = lax.all_to_all(outgoing, "ep", split_axis=0, concat_axis=0, tiled=True)
    gate_part = jnp.einsum("scd,df->scf", arrived_rows, w_gate, preferred_element_type=jnp.float32)
    up_part = jnp.einsum("scd,df->scf", arrived_rows, w_up, preferred_element_type=jnp.float32)
    hidden = (jax.nn.silu(gate_part) * up_part).astype(jnp.bfloat16)
    expert_out = jnp.einsum(
        "scf,fd->scd",
        lax.all_gather(hidden, "tp", axis=2, tiled=True),
        w_down,
        preferred_element_type=jnp.float32,
    ).astype(jnp.bfloat16)
    returned = lax.all_to_all(expert_out, "ep", split_axis=0, concat_axis=0, tiled=True)
    picked = returned.reshape(experts * capacity, -1)[target].reshape(row_count, 2, -1)
    return jnp.sum(picked.astype(jnp.float32) * route_weights[:, :, None], axis=1).astype(
        jnp.bfloat16
    )


def on_device(
    queries,
    keys,
    values,
    gates,
    log_decay,
    out_weight,
    moe_rows,
    moe_gain,
    routes,
    route_weights,
    gate_proj,
    up_proj,
    down_proj,
):
    mixer_out = retention_half(queries, keys, values, gates, log_decay, out_weight)
    moe_out = expert_half(moe_rows, moe_gain, routes, route_weights, gate_proj, up_proj, down_proj)
    return (mixer_out, moe_out)


def solution(mesh):
    placed = (
        P("ep", "tp"),
        P("ep", "tp"),
        P("ep", "tp"),
        P("ep", "tp"),
        P("ep", "tp"),
        P(None, "tp"),
        P("ep", None),
        P(),
        P("ep", None),
        P("ep", None),
        P("ep", None, "tp"),
        P("ep", None, "tp"),
        P("ep", None, "tp"),
    )
    return jax.shard_map(
        on_device,
        mesh=mesh,
        in_specs=placed,
        out_specs=(P("ep", "tp"), P("ep", "tp")),
        check_vma=False,
    )
```

profile of v0, /device:TPU:0, one launch (start us, length us, event | category | flops | bytes accessed | tf_op | source)
XLA Modules:
  0.0 199.5 jit_solution(13536535929649242897)
XLA Ops:
  7.2 1.0 copy.86
  8.4 0.7 broadcast_multiply_fusion
  9.1 1.1 reduce-window.6
  10.3 0.2 slice_reduce_fusion
  10.9 2.4 %scatter_custom_fusion = s32[512]{0:T(512)S(1)} fusion(s32[512]{0:T(512)S(1)} %bitcast.110, s32[512]{0:T(512)S(1)} %add_select_fusion, s32[]{:T(128)} %copy.125), kind=kCustom, calls=%fused_computation.90 | custom fusion | bytes 2052 | tf_op jit(solution)/shard_map/scatter | solution.py:125
  13.4 0.7 convert_element_type.72
  14.1 1.5 fusion.9
  15.6 1.5 fusion.11
  17.2 3.3 %gather_fusion = bf16[512,2048]{1,0:T(8,128)(2,1)} fusion(bf16[256,2048]{1,0:T(8,128)(2,1)S(1)} %fusion.11, s32[1024]{0:T(1024)S(1)} %pad_clamp_fusion.1), kind=kCustom, calls=%fused_computation | custom fusion | bytes 4196352 | tf_op jit(solution)/shard_map/gather | solution.py:127
  20.5 6.5 %all-to-all-start = ((bf16[8,64,2048]{2,1,0:T(8,128)(2,1)}), bf16[8,64,2048]{2,1,0:T(8,128)(2,1)}, u32[]{:S(2)}, u32[]{:S(2)}) async-start(bf16[8,64,2048]{2,1,0:T(8,128)(2,1)} %bitcast.100), calls=%async_computation | async-start | bytes 4194304 | tf_op jit(solution)/shard_map/all_to_all | solution.py:131
  27.2 1.1 copy.93
  28.3 0.3 multiply_cosine_fusion
  28.6 1.0 subtract_convert_fusion
  29.6 1.1 concatenate.20
  30.7 0.2 copy.72
  30.9 1.8 concatenate.21
  32.7 1.1 copy.73
  33.8 0.8 copy.91
  34.6 1.1 reduce_window_sum.37
  35.7 0.7 fusion.56
  36.5 1.0 copy.78
  37.5 1.7 reshape.218
  39.2 0.2 fusion.24
  39.4 0.7 copy-done.2
  40.1 1.7 fusion.27
  41.8 1.7 while.29
  41.8 0.7 bitcast_dynamic-update-slice_fusion.3
  42.7 0.7 bitcast_dynamic-update-slice_fusion.3
  43.5 0.7 copy-done.1
  44.3 48.7 %all-to-all-done = bf16[8,64,2048]{2,1,0:T(8,128)(2,1)} async-done(((bf16[8,64,2048]{2,1,0:T(8,128)(2,1)}), bf16[8,64,2048]{2,1,0:T(8,128)(2,1)}, u32[]{:S(2)}, u32[]{:S(2)}) %all-to-all-start) | async-done | bytes 2097184 | tf_op jit(solution)/shard_map/all_to_all | solution.py:131
  92.9 5.3 %fusion.7 = f32[8,64,1024]{2,1,0:T(8,128)S(1)} fusion(bf16[8,64,2048]{2,1,0:T(8,128)(2,1)} %all-to-all-done, bf16[1,2048,1024]{2,1,0:T(8,128)(2,1)} %param.27), kind=kOutput, calls=%fused_computation.15 | convolution fusion | flops 2147483648 | bytes 8388608 | tf_op jit(solution)/shard_map/scd,df->scf/dot_general | solution.py:132
  98.3 5.2 %multiply_convert_fusion = bf16[8,64,1024]{2,1,0:T(8,128)(2,1)} fusion(f32[8,64,1024]{2,1,0:T(8,128)S(1)} %fusion.7, bf16[8,64,2048]{2,1,0:T(8,128)(2,1)} %all-to-all-done, bf16[1,2048,1024]{2,1,0:T(8,128)(2,1)S(1)} %copy-done.11), kind=kOutput, calls=%fused_computation.22 | convolution fusion | flops 2150629376 | bytes 9437184 | tf_op jit(solution)/shard_map/scd,df->scf/dot_general | solution.py:133
  103.6 0.6 dynamic-slice
  105.0 14.7 %all-reduce = f32[32]{0:T(128)S(1)} all-reduce(f32[32]{0:T(128)S(1)} %exponential_dynamic-update-slice_fusion), channel_id=2, replica_groups=mesh['ep'=8,'tp'=4] {'ep'}, use_global_device_ids=true, to_apply=%add | all-reduce | flops 32 | bytes 256
  119.8 0.7 reshape.252
  120.5 0.2 copy.68
  121.2 12.4 %while.30 = (s32[]{:T(128)}, f32[4,128,128]{2,1,0:T(8,128)S(1)}, s32[]{:T(128)}, f32[8,4]{1,0:T(8,128)}, f32[8,4,128,128]{3,2,1,0:T(8,128)}) while((s32[]{:T(128)}, f32[4,128,128]{2,1,0:T(8,128)S(1)}, s32[]{:T(128)}, f32[8,4]{1,0:T(8,128)}, f32[8,4,128,128]{3,2,1,0:T(8,128)}) %tuple.79), condition=%wide.region_6.7_spmd.clone.clone, body=%wide.region_5.6_spmd.clone.sunk.clone | while | flops 262148 | bytes 786569 | solution.py:20
  121.2 0.7 dynamic-slice_bitcast_fusion.3
  121.9 1.0 fusion.68
  123.0 0.7 dynamic-slice_bitcast_fusion.3
  123.7 1.0 fusion.68
  124.8 0.7 dynamic-slice_bitcast_fusion.3
  125.4 1.0 fusion.68
  126.5 0.7 dynamic-slice_bitcast_fusion.3
  127.2 1.0 fusion.68
  128.3 0.7 dynamic-slice_bitcast_fusion.3
  128.9 1.0 fusion.68
  130.0 0.7 dynamic-slice_bitcast_fusion.3
  130.7 1.1 fusion.68
  131.8 0.7 dynamic-slice_bitcast_fusion.3
  132.5 1.0 fusion.68
  133.6 2.5 %fusion.18 = f32[2,128,4,128]{1,3,2,0:T(8,128)} fusion(f32[2,4,128,128]{3,2,1,0:T(8,128)} %get-tuple-element.124, f32[2,128,4]{1,2,0:T(4,128)S(1)} %copy.82, f32[4,128,128]{2,1,0:T(8,128)S(1)} %get-tuple-element.126, f32[2,4]{1,0:T(2,128)S(1)} %subtract_exponential_fusion.1, bf16[2,128,4,64]{3,1,2,0:T(8,128)(2,1)S(1)} %copy.69, ...), kind=kOutput, calls=%fused_computation.28 | convolution fusion | flops 202244096 | bytes 1576992 | tf_op jit(solution)/shard_map/nihd,nhde->nihe/dot_general | solution.py:88
  136.1 2.4 %multiply_reduce_fusion.1 = (f32[2,128,4]{1,2,0:T(4,128)S(1)}, f32[2,128,4,128]{1,3,2,0:T(8,128)}) fusion(f32[2,128,4,128]{1,3,2,0:T(8,128)} %fusion.18, bf16[2,128,4,128]{3,2,1,0:T(4,128)(2,1)S(1)} %copy-done.4, bf16[2,128,4,128]{3,1,2,0:T(8,128)(2,1)S(1)} %copy-done.3, f32[2,4,128]{2,1,0:T(4,128)S(1)} %copy.75, ...), kind=kOutput, calls=%fused_computation.41 | convolution fusion | flops 68680704 | bytes 1859584 | tf_op jit(solution)/shard_map/nhij,njhd->nihd/dot_general | solution.py:69
  138.7 1.3 copy.83
  140.0 0.3 mul.255
  140.3 1.8 fusion.34
  142.2 13.0 %all-gather.8.cloned.1.call-done = bf16[8,64,4096]{2,1,0:T(8,128)(2,1)} async-done(((bf16[8,64,1024]{2,1,0:T(8,128)(2,1)}), bf16[8,64,4096]{2,1,0:T(8,128)(2,1)}) %all-gather.8.cloned.1.call-update) | async-done | bytes 4194320 | tf_op jit(solution)/shard_map/all_gather | solution.py:137
  155.2 6.6 %fusion.14 = bf16[8,64,512]{2,1,0:T(8,128)(2,1)} fusion(bf16[8,64,4096]{2,1,0:T(8,128)(2,1)} %all-gather.8.cloned.1.call-done, bf16[1,4096,512]{2,1,0:T(8,128)(2,1)} %param.29), kind=kOutput, calls=%fused_computation.23 | convolution fusion | flops 2147745792 | bytes 8912896 | tf_op jit(solution)/shard_map/scf,fd->scd/dot_general | solution.py:135
  161.8 4.6 %all-to-all-start.1 = ((bf16[8,64,512]{2,1,0:T(8,128)(2,1)}), bf16[8,64,512]{2,1,0:T(8,128)(2,1)S(1)}, u32[]{:S(2)}, u32[]{:S(2)}) async-start(bf16[8,64,512]{2,1,0:T(8,128)(2,1)} %fusion.14), calls=%async_computation.1 | async-start | bytes 1048576 | tf_op jit(solution)/shard_map/all_to_all | solution.py:141
  166.5 17.4 %all-gather.6.cloned.1.call-done = bf16[256,2048]{1,0:T(8,128)(2,1)} async-done(((bf16[256,512]{1,0:T(8,128)(2,1)}), bf16[256,2048]{1,0:T(8,128)(2,1)}) %all-gather.6.cloned.1.call-update) | async-done | bytes 1048592 | tf_op jit(solution)/shard_map/all_gather | solution.py:101
  184.0 2.6 %convolution_convert_fusion = bf16[256,512]{1,0:T(8,128)(2,1)} fusion(bf16[256,2048]{1,0:T(8,128)(2,1)} %all-gather.6.cloned.1.call-done, bf16[2048,512]{1,0:T(8,128)(2,1)S(1)} %copy-done), kind=kOutput, calls=%fused_computation.29 | convolution fusion | flops 537001984 | bytes 3407872 | tf_op jit(solution)/shard_map/dot_general | solution.py:100
  186.6 2.6 %gather_fusion.1 = bf16[512,512]{1,0:T(8,128)(2,1)} fusion(bf16[512,512]{1,0:T(8,128)(2,1)S(1)} %bitcast.99, s32[1024]{0:T(1024)S(1)} %pad_clamp_fusion), kind=kCustom, calls=%fused_computation.1 | custom fusion | bytes 1050624 | tf_op jit(solution)/shard_map/gather | solution.py:142
  189.2 1.7 reshape.227
  190.9 2.1 %multiply_reduce_fusion = bf16[256,512]{1,0:T(8,128)(2,1)} fusion(f32[256,2,512]{2,1,0:T(2,128)S(1)} %reshape.227, f32[256,2]{1,0:T(8,128)S(1)} %copy.88), kind=kLoop, calls=%fused_computation.31 | loop fusion | flops 393216 | bytes 1312768 | tf_op jit(solution)/shard_map/reduce_sum | solution.py:143
  (70 shorter events, 2.2 us)
Async XLA Ops:
  7.2 176.8 %copy-start = (bf16[2048,512]{1,0:T(8,128)(2,1)S(1)}, bf16[2048,512]{1,0:T(8,128)(2,1)}, u32[]{:S(2)}) copy-start(bf16[2048,512]{1,0:T(8,128)(2,1)} %param.22) | copy-start | bytes 6291460
  20.5 6.6 %copy-start.8 = (bf16[256,512]{1,0:T(8,128)(2,1)S(1)}, bf16[256,512]{1,0:T(8,128)(2,1)}, u32[]{:S(2)}) copy-start(bf16[256,512]{1,0:T(8,128)(2,1)} %param.17) | copy-start | bytes 786436
  20.5 72.5 %all-to-all-start = ((bf16[8,64,2048]{2,1,0:T(8,128)(2,1)}), bf16[8,64,2048]{2,1,0:T(8,128)(2,1)}, u32[]{:S(2)}, u32[]{:S(2)}) async-start(bf16[8,64,2048]{2,1,0:T(8,128)(2,1)} %bitcast.100), calls=%async_computation | async-start | bytes 4194304 | tf_op jit(solution)/shard_map/all_to_all | solution.py:131
  26.9 94.2 %all-gather.10.cloned.1.call-start = ((), (), s32[]{:S(2)}) async-start(), calls=%async_computation.4 | async-start | bytes 2359296 | tf_op jit(solution)/shard_map/all_gather | solution.py:11
  28.6 5.2 %copy-start.9 = (f32[256,4]{0,1:T(4,128)S(1)}, f32[256,4]{0,1:T(4,128)}, u32[]{:S(2)}) copy-start(f32[256,4]{0,1:T(4,128)} %param.21) | copy-start | bytes 12292
  39.4 0.7 copy-start.2
  43.5 0.7 copy-start.1
  44.2 110.9 %all-gather.8.cloned.1.call-start = ((), (), s32[]{:S(2)}) async-start(), calls=%async_computation.3 | async-start | bytes 5242880 | tf_op jit(solution)/shard_map/all_gather | solution.py:137
  92.9 5.3 %copy-start.11 = (bf16[1,2048,1024]{2,1,0:T(8,128)(2,1)S(1)}, bf16[1,2048,1024]{2,1,0:T(8,128)(2,1)}, u32[]{:S(2)}) copy-start(bf16[1,2048,1024]{2,1,0:T(8,128)(2,1)} %param.28) | copy-start | bytes 12582916
  98.2 5.4 %copy-start.12 = (u32[32]{0:T(128)S(1)}, u32[32]{0:T(128)}, u32[]{:S(2)}) copy-start(u32[32]{0:T(128)} %constant.105) | copy-start | bytes 388
  98.3 22.2 %copy-start.7 = (bf16[256,4,64]{0,2,1:T(8,128)(2,1)S(1)}, bf16[256,4,64]{0,2,1:T(8,128)(2,1)}, u32[]{:S(2)}) copy-start(bf16[256,4,64]{0,2,1:T(8,128)(2,1)} %get-tuple-element.183) | copy-start | bytes 393220
  98.3 22.4 %copy-start.6 = (bf16[256,4,64]{0,2,1:T(8,128)(2,1)S(1)}, bf16[256,4,64]{0,2,1:T(8,128)(2,1)}, u32[]{:S(2)}) copy-start(bf16[256,4,64]{0,2,1:T(8,128)(2,1)} %get-tuple-element.184) | copy-start | bytes 393220
  103.5 17.5 %copy-start.5 = (f32[2,128,4]{2,1,0:T(8,128)S(1)}, f32[2,128,4]{2,1,0:T(8,128)}, u32[]{:S(2)}) copy-start(f32[2,128,4]{2,1,0:T(8,128)} %get-tuple-element.191) | copy-start | bytes 12292
  103.5 80.5 %all-gather.6.cloned.1.call-start = ((), (), s32[]{:S(2)}) async-start(), calls=%async_computation.2 | async-start | bytes 1310720 | tf_op jit(solution)/shard_map/all_gather | solution.py:101
  121.2 14.9 %copy-start.3 = (bf16[2,128,4,128]{3,1,2,0:T(8,128)(2,1)S(1)}, bf16[2,128,4,128]{3,1,2,0:T(8,128)(2,1)}, u32[]{:S(2)}) copy-start(bf16[2,128,4,128]{3,1,2,0:T(8,128)(2,1)} %copy-done.2) | copy-start | bytes 786436
  121.2 14.9 %copy-start.4 = (bf16[2,128,4,128]{3,2,1,0:T(4,128)(2,1)S(1)}, bf16[2,128,4,128]{3,2,1,0:T(4,128)(2,1)}, u32[]{:S(2)}) copy-start(bf16[2,128,4,128]{3,2,1,0:T(4,128)(2,1)} %reshape.218) | copy-start | bytes 786436
  142.2 24.2 %copy-start.10 = (f32[256,2]{0,1:T(2,128)S(1)}, f32[256,2]{0,1:T(2,128)}, u32[]{:S(2)}) copy-start(f32[256,2]{0,1:T(2,128)} %param.26) | copy-start | bytes 6148
  161.8 24.8 %all-to-all-start.1 = ((bf16[8,64,512]{2,1,0:T(8,128)(2,1)}), bf16[8,64,512]{2,1,0:T(8,128)(2,1)S(1)}, u32[]{:S(2)}, u32[]{:S(2)}) async-start(bf16[8,64,512]{2,1,0:T(8,128)(2,1)} %fusion.14), calls=%async_computation.1 | async-start | bytes 1048576 | tf_op jit(solution)/shard_map/all_to_all | solution.py:141
Sparse Core Ops, SparseCore 0:
  44.3 48.1 all-gather.9
  103.6 51.5 all-gather.7
  157.6 26.3 all-gather.5
where the time goes:
time: 201 us; the launch traced here: 200 us
  waiting for transfers between devices  79.1 us (39%)
  local copies, waits for them, and re-layouts  30.9 us (15%)
  matrix products  26.4 us (13%)
  other arithmetic  22.1 us (11%)
  between operations  14.8 us (7%)
  blocking collectives  14.7 us (7%)
  starting transfers between devices  11.2 us (6%)
    all_to_all x1, waiting for transfers between devices, expert_half(): lax.all_to_all(outgoing, 'ep', split_axis=0, concat_axis=0, tiled=True)  48.7 us
    all_gather x1, waiting for transfers between devices, retention_half(): lax.all_gather(head_out, 'tp', axis=1, tiled=True)  17.4 us
    unnamed x1, blocking collectives  14.7 us
    all_gather x1, waiting for transfers between devices, expert_half(): lax.all_gather(hidden, 'tp', axis=2, tiled=True)  13 us
    select_n x7, other arithmetic, turn(): jnp.where(position < mine, new, old)  7.41 us
    dot_general x1, matrix products, expert_half(): jnp.einsum('scf,fd->scd', lax.all_gather(hidden, 'tp', axis=2, tiled=True...  6.6 us
    all_to_all x1, starting transfers between devices, expert_half(): lax.all_to_all(outgoing, 'ep', split_axis=0, concat_axis=0, tiled=True)  6.49 us
    dot_general x1, matrix products, expert_half(): jnp.einsum('scd,df->scf', arrived_rows, w_gate, preferred_element_type=jn...  5.3 us
  transfers between devices with their start and end apart: 5, of which 3 were waited for; matrix products, arithmetic and copies ran while one was open for 29% of the time, Pallas kernels for 0%

commit v1 on v0

--- a/solution.py
+++ b/solution.py
@@ -4,6 +4,22 @@
 from jax.sharding import PartitionSpec as P
 
 BLOCK = 128
+
+
+def product_in_turn(value, axis, dim, contribution):
+    size, index, rows = (lax.axis_size(axis), lax.axis_index(axis), value.shape[dim])
+    forward = [(i, (i + 1) % size) for i in range(size)]
+    left = [(i, (i - 1) % size) for i in range(size)]
+    middle = size // 2
+    from_left = from_right = value
+    so_far = contribution(value, index * rows)
+    for turn in range(1, middle + 1):
+        from_left = lax.ppermute(from_left, axis, forward)
+        if turn < size - middle:
+            from_right = lax.ppermute(from_right, axis, left)
+            so_far = so_far + contribution(from_right, (index + turn) % size * rows)
+        so_far = so_far + contribution(from_left, (index - turn) % size * rows)
+    return so_far
 
 
 def carried_in(value, axis, join, neutral):
@@ -132,11 +148,16 @@
     gate_part = jnp.einsum("scd,df->scf", arrived_rows, w_gate, preferred_element_type=jnp.float32)
     up_part = jnp.einsum("scd,df->scf", arrived_rows, w_up, preferred_element_type=jnp.float32)
     hidden = (jax.nn.silu(gate_part) * up_part).astype(jnp.bfloat16)
-    expert_out = jnp.einsum(
-        "scf,fd->scd",
-        lax.all_gather(hidden, "tp", axis=2, tiled=True),
-        w_down,
-        preferred_element_type=jnp.float32,
+    expert_out = product_in_turn(
+        hidden,
+        "tp",
+        2,
+        lambda part_2, offset: jnp.einsum(
+            "scf,fd->scd",
+            part_2,
+            lax.dynamic_slice_in_dim(w_down, offset, part_2.shape[2], axis=0),
+            preferred_element_type=jnp.float32,
+        ),
     ).astype(jnp.bfloat16)
     returned = lax.all_to_all(expert_out, "ep", split_axis=0, concat_axis=0, tiled=True)
     picked = returned.reshape(experts * capacity, -1)[target].reshape(row_count, 2, -1)

time: 201 us -> 225 us (1.12)
  blocking collectives: 14.7 us -> 35.2 us
  waiting for transfers between devices: 79.1 us -> 64.9 us
  starting transfers between devices: 11.2 us -> 25.2 us
  matrix products: 26.4 us -> 29.1 us
    ppermute x0 -> x3, waiting for transfers between devices: none -> 41.7 us  [the longest x2 41.7 us: product_in_turn(): from_left = lax.ppermute(from_left, axis, forward)]
    all_to_all x1, waiting for transfers between devices: 48.7 us -> 10.6 us  [expert_half(): lax.all_to_all(outgoing, 'ep', split_axis=0, concat_axis=0, tiled=True)]
    unnamed x1, blocking collectives: 14.7 us -> 35.2 us
    all_gather x1, waiting for transfers between devices: 17.4 us -> 0.02 us  [retention_half(): lax.all_gather(head_out, 'tp', axis=1, tiled=True)]
    all_gather x1 -> x0, waiting for transfers between devices: 13 us -> none  [expert_half(): lax.all_gather(hidden, 'tp', axis=2, tiled=True)]
    all_to_all x1, waiting for transfers between devices: 0.01 us -> 12.5 us  [expert_half(): lax.all_to_all(expert_out, 'ep', split_axis=0, concat_axis=0, tiled=True)]
    all_to_all x1, starting transfers between devices: 4.61 us -> 14.7 us  [expert_half(): lax.all_to_all(expert_out, 'ep', split_axis=0, concat_axis=0, tiled=True)]
    ppermute x0 -> x3, starting transfers between devices: none -> 3.93 us  [the longest x1 2.44 us: product_in_turn(): from_right = lax.ppermute(from_right, axis, left)]
  transfers between devices with their start and end apart: 5 -> 7, of which waited for: 3 -> 4; matrix products, arithmetic and copies ran while one was open for 29% -> 27% of each run, Pallas kernels for 0% -> 0%
where the time goes in v1:
time: 225 us; the launch traced here: 223 us
  waiting for transfers between devices  64.9 us (29%)
  blocking collectives  35.2 us (16%)
  local copies, waits for them, and re-layouts  31.4 us (14%)
  matrix products  29.1 us (13%)
  starting transfers between devices  25.2 us (11%)
  other arithmetic  22 us (10%)
  between operations  15.2 us (7%)
    ppermute x2, waiting for transfers between devices, product_in_turn(): from_left = lax.ppermute(from_left, axis, forward)  41.7 us
    unnamed x1, blocking collectives  35.2 us
    all_to_all x1, starting transfers between devices, expert_half(): lax.all_to_all(expert_out, 'ep', split_axis=0, concat_axis=0, tiled=True)  14.7 us
    all_to_all x1, waiting for transfers between devices, expert_half(): lax.all_to_all(expert_out, 'ep', split_axis=0, concat_axis=0, tiled=True)  12.5 us
    all_to_all x1, waiting for transfers between devices, expert_half(): lax.all_to_all(outgoing, 'ep', split_axis=0, concat_axis=0, tiled=True)  10.6 us
    dot_general x4, matrix products, expert_half(): jnp.einsum('scf,fd->scd', part_2, lax.dynamic_slice_in_dim(w_down, offset...  9.31 us
    select_n x7, other arithmetic, turn(): jnp.where(position < mine, new, old)  7.34 us
    all_to_all x1, starting transfers between devices, expert_half(): lax.all_to_all(outgoing, 'ep', split_axis=0, concat_axis=0, tiled=True)  6.49 us
  transfers between devices with their start and end apart: 7, of which 4 were waited for; matrix products, arithmetic and copies ran while one was open for 27% of the time, Pallas kernels for 0%

profile of v1, /device:TPU:0, one launch (start us, length us, event | category | flops | bytes accessed | tf_op | source)
XLA Modules:
  0.0 223.3 jit_solution(7353413640624568495)
XLA Ops:
  7.2 1.0 copy.86
  8.4 0.7 broadcast_multiply_fusion
  9.1 1.1 reduce-window.6
  10.9 2.4 %scatter_custom_fusion = s32[512]{0:T(512)S(1)} fusion(s32[512]{0:T(512)S(1)} %bitcast.123, s32[512]{0:T(512)S(1)} %add_select_fusion, s32[]{:T(128)} %copy.125), kind=kCustom, calls=%fused_computation.100 | custom fusion | bytes 2052 | tf_op jit(solution)/shard_map/scatter | solution.py:141
  13.4 0.7 convert_element_type.72
  14.1 1.5 fusion.7
  15.6 1.5 fusion.9
  17.2 3.3 %gather_fusion = bf16[512,2048]{1,0:T(8,128)(2,1)} fusion(bf16[256,2048]{1,0:T(8,128)(2,1)S(1)} %fusion.9, s32[1024]{0:T(1024)S(1)} %pad_clamp_fusion.1), kind=kCustom, calls=%fused_computation | custom fusion | bytes 4196352 | tf_op jit(solution)/shard_map/gather | solution.py:143
  20.5 6.5 %all-to-all-start = ((bf16[8,64,2048]{2,1,0:T(8,128)(2,1)}), bf16[8,64,2048]{2,1,0:T(8,128)(2,1)}, u32[]{:S(2)}, u32[]{:S(2)}) async-start(bf16[8,64,2048]{2,1,0:T(8,128)(2,1)} %bitcast.113), calls=%async_computation | async-start | bytes 4194304 | tf_op jit(solution)/shard_map/all_to_all | solution.py:147
  27.2 1.1 copy.93
  28.6 1.0 subtract_convert_fusion
  29.6 1.1 concatenate.20
  30.9 1.8 concatenate.21
  32.7 1.1 copy.73
  33.8 0.8 copy.91
  34.6 1.1 reduce_window_sum.37
  35.7 0.7 fusion.65
  36.5 1.0 copy.78
  37.5 1.7 reshape.222
  39.4 0.7 copy-done.3
  40.1 1.7 fusion.32
  41.9 1.7 while.29
  41.9 0.7 bitcast_dynamic-update-slice_fusion.3
  42.7 0.7 bitcast_dynamic-update-slice_fusion.3
  43.6 0.7 copy-done.1
  44.5 0.7 dynamic-slice.4
  45.9 35.2 %all-reduce = f32[32]{0:T(128)S(1)} all-reduce(f32[32]{0:T(128)S(1)} %exponential_dynamic-update-slice_fusion), channel_id=2, replica_groups=mesh['ep'=8,'tp'=4] {'ep'}, use_global_device_ids=true, to_apply=%add | all-reduce | flops 32 | bytes 256
  81.1 0.7 reshape.256
  82.5 10.6 %all-to-all-done = bf16[8,64,2048]{2,1,0:T(8,128)(2,1)} async-done(((bf16[8,64,2048]{2,1,0:T(8,128)(2,1)}), bf16[8,64,2048]{2,1,0:T(8,128)(2,1)}, u32[]{:S(2)}, u32[]{:S(2)}) %all-to-all-start) | async-done | bytes 2097184 | tf_op jit(solution)/shard_map/all_to_all | solution.py:147
  93.1 5.3 %fusion.5 = f32[8,64,1024]{2,1,0:T(8,128)S(1)} fusion(bf16[8,64,2048]{2,1,0:T(8,128)(2,1)} %all-to-all-done, bf16[1,2048,1024]{2,1,0:T(8,128)(2,1)} %param.27), kind=kOutput, calls=%fused_computation.13 | convolution fusion | flops 2147483648 | bytes 8388608 | tf_op jit(solution)/shard_map/scd,df->scf/dot_general | solution.py:148
  98.4 5.1 %multiply_convert_fusion = bf16[8,64,1024]{2,1,0:T(8,128)(2,1)} fusion(f32[8,64,1024]{2,1,0:T(8,128)S(1)} %fusion.5, bf16[8,64,2048]{2,1,0:T(8,128)(2,1)} %all-to-all-done, bf16[1,2048,1024]{2,1,0:T(8,128)(2,1)S(1)} %copy-done.12), kind=kOutput, calls=%fused_computation.20 | convolution fusion | flops 2150629376 | bytes 9437184 | tf_op jit(solution)/shard_map/scd,df->scf/dot_general | solution.py:149
  103.5 2.4 %collective-permute-start = (bf16[8,64,1024]{2,1,0:T(8,128)(2,1)}, bf16[8,64,1024]{2,1,0:T(8,128)(2,1)}, u32[]{:S(2)}, u32[]{:S(2)}) collective-permute-start(bf16[8,64,1024]{2,1,0:T(8,128)(2,1)} %multiply_convert_fusion), channel_id=1, source_target_pairs={{0,3},{1,0},{2,1},{3,2},{4,7},{5,4},{6,5},{7,6},{8,11},{9,8},{10,9... | collective-permute-start | bytes 3145736 | tf_op jit(solution)/shard_map/ppermute | solution.py:19
  106.0 12.4 %while.30 = (s32[]{:T(128)}, f32[4,128,128]{2,1,0:T(8,128)S(1)}, s32[]{:T(128)}, f32[8,4]{1,0:T(8,128)}, f32[8,4,128,128]{3,2,1,0:T(8,128)}) while((s32[]{:T(128)}, f32[4,128,128]{2,1,0:T(8,128)S(1)}, s32[]{:T(128)}, f32[8,4]{1,0:T(8,128)}, f32[8,4,128,128]{3,2,1,0:T(8,128)}) %tuple.77), condition=%wide.region_6.7_spmd.clone.clone, body=%wide.region_5.6_spmd.clone.sunk.clone | while | flops 262148 | bytes 786569 | solution.py:36
  106.0 0.7 dynamic-slice_bitcast_fusion.3
  106.8 1.0 fusion.80
  107.8 0.7 dynamic-slice_bitcast_fusion.3
  108.5 1.0 fusion.80
  109.6 0.7 dynamic-slice_bitcast_fusion.3
  110.3 1.0 fusion.80
  111.4 0.7 dynamic-slice_bitcast_fusion.3
  112.0 1.0 fusion.80
  113.1 0.7 dynamic-slice_bitcast_fusion.3
  113.8 1.0 fusion.80
  114.9 0.7 dynamic-slice_bitcast_fusion.3
  115.6 1.0 fusion.80
  116.6 0.7 dynamic-slice_bitcast_fusion.3
  117.3 1.0 fusion.80
  118.4 2.6 %fusion.14 = f32[2,128,4,128]{1,3,2,0:T(8,128)} fusion(f32[2,4,128,128]{3,2,1,0:T(8,128)} %get-tuple-element.124, f32[2,128,4]{1,2,0:T(4,128)S(1)} %copy.82, f32[4,128,128]{2,1,0:T(8,128)S(1)} %get-tuple-element.126, f32[2,4]{1,0:T(2,128)S(1)} %subtract_exponential_fusion.1, bf16[2,128,4,64]{3,1,2,0:T(8,128)(2,1)S(1)} %copy.69, ...), kind=kOutput, calls=%fused_computation.29 | convolution fusion | flops 202244096 | bytes 1576992 | tf_op jit(solution)/shard_map/nihd,nhde->nihe/dot_general | solution.py:104
  120.9 2.4 %multiply_reduce_fusion.1 = (f32[2,128,4]{1,2,0:T(4,128)S(1)}, f32[2,128,4,128]{1,3,2,0:T(8,128)}) fusion(f32[2,128,4,128]{1,3,2,0:T(8,128)} %fusion.14, bf16[2,128,4,128]{3,2,1,0:T(4,128)(2,1)S(1)} %copy-done.5, bf16[2,128,4,128]{3,1,2,0:T(8,128)(2,1)S(1)} %copy-done.4, f32[2,4,128]{2,1,0:T(4,128)S(1)} %copy.75, ...), kind=kOutput, calls=%fused_computation.51 | convolution fusion | flops 68680704 | bytes 1859584 | tf_op jit(solution)/shard_map/nhij,njhd->nihd/dot_general | solution.py:85
  123.6 1.3 copy.83
  124.8 24.9 %collective-permute-done.1 = bf16[8,64,1024]{2,1,0:T(8,128)(2,1)} collective-permute-done((bf16[8,64,1024]{2,1,0:T(8,128)(2,1)}, bf16[8,64,1024]{2,1,0:T(8,128)(2,1)}, u32[]{:S(2)}, u32[]{:S(2)}) %collective-permute-start.1) | collective-permute-done | bytes 1048608 | tf_op jit(solution)/shard_map/ppermute | solution.py:17
  149.7 1.5 collective-permute-start.2
  151.5 1.8 fusion.39
  153.4 2.3 %fusion.19 = f32[8,64,512]{2,1,0:T(8,128)S(1)} fusion(bf16[8,64,1024]{2,1,0:T(8,128)(2,1)} %multiply_convert_fusion, bf16[1,4096,512]{2,1,0:T(8,128)(2,1)} %param.29, s32[]{:T(128)S(6)} %select_n.80), kind=kOutput, calls=%fused_computation.35 | convolution fusion | flops 536870912 | bytes 3145732 | tf_op jit(solution)/shard_map/scf,fd->scd/dot_general | solution.py:155
  155.7 2.4 %convolution_add_fusion.2 = f32[8,64,512]{2,1,0:T(8,128)S(1)} fusion(f32[8,64,512]{2,1,0:T(8,128)S(1)} %fusion.19, bf16[8,64,1024]{2,1,0:T(8,128)(2,1)} %collective-permute-done, bf16[1,4096,512]{2,1,0:T(8,128)(2,1)} %param.29, s32[]{:T(128)S(6)} %select_n.82), kind=kOutput, calls=%fused_computation.23 | convolution fusion | flops 537133056 | bytes 4194308 | tf_op jit(solution)/shard_map/scf,fd->scd/dot_general | solution.py:155
  158.5 1.9 convolution_add_fusion.1
  160.4 16.9 %collective-permute-done.2 = bf16[8,64,1024]{2,1,0:T(8,128)(2,1)} collective-permute-done((bf16[8,64,1024]{2,1,0:T(8,128)(2,1)}, bf16[8,64,1024]{2,1,0:T(8,128)(2,1)}, u32[]{:S(2)}, u32[]{:S(2)}) %collective-permute-start.2) | collective-permute-done | bytes 1048608 | tf_op jit(solution)/shard_map/ppermute | solution.py:17
  177.3 2.7 %fusion.12 = bf16[8,64,512]{2,1,0:T(8,128)(2,1)} fusion(f32[8,64,512]{2,1,0:T(8,128)S(1)} %convolution_add_fusion.1, bf16[8,64,1024]{2,1,0:T(8,128)(2,1)} %collective-permute-done.2, bf16[1,4096,512]{2,1,0:T(8,128)(2,1)S(1)} %copy-done.2, s32[]{:T(128)S(6)} %select_n.86), kind=kOutput, calls=%fused_computation.24 | convolution fusion | flops 537395200 | bytes 3670020 | tf_op jit(solution)/shard_map/scf,fd->scd/dot_general | solution.py:155
  180.0 14.7 %all-to-all-start.1 = ((bf16[8,64,512]{2,1,0:T(8,128)(2,1)}), bf16[8,64,512]{2,1,0:T(8,128)(2,1)S(1)}, u32[]{:S(2)}, u32[]{:S(2)}) async-start(bf16[8,64,512]{2,1,0:T(8,128)(2,1)} %fusion.12), calls=%async_computation.1 | async-start | bytes 1048576 | tf_op jit(solution)/shard_map/all_to_all | solution.py:162
  194.9 2.6 %convolution_convert_fusion = bf16[256,512]{1,0:T(8,128)(2,1)} fusion(bf16[256,2048]{1,0:T(8,128)(2,1)} %all-gather.5.cloned.1.call-done, bf16[2048,512]{1,0:T(8,128)(2,1)S(1)} %copy-done), kind=kOutput, calls=%fused_computation.30 | convolution fusion | flops 537001984 | bytes 3407872 | tf_op jit(solution)/shard_map/dot_general | solution.py:116
  197.6 12.5 %all-to-all-done.1 = bf16[8,64,512]{2,1,0:T(8,128)(2,1)S(1)} async-done(((bf16[8,64,512]{2,1,0:T(8,128)(2,1)}), bf16[8,64,512]{2,1,0:T(8,128)(2,1)S(1)}, u32[]{:S(2)}, u32[]{:S(2)}) %all-to-all-start.1) | async-done | bytes 524320 | tf_op jit(solution)/shard_map/all_to_all | solution.py:162
  210.1 2.6 %gather_fusion.1 = bf16[512,512]{1,0:T(8,128)(2,1)} fusion(bf16[512,512]{1,0:T(8,128)(2,1)S(1)} %bitcast.112, s32[1024]{0:T(1024)S(1)} %pad_clamp_fusion), kind=kCustom, calls=%fused_computation.1 | custom fusion | bytes 1050624 | tf_op jit(solution)/shard_map/gather | solution.py:163
  212.7 1.7 reshape.231
  214.4 2.1 multiply_reduce_fusion
  (78 shorter events, 4.0 us)
Async XLA Ops:
  7.2 187.8 %copy-start = (bf16[2048,512]{1,0:T(8,128)(2,1)S(1)}, bf16[2048,512]{1,0:T(8,128)(2,1)}, u32[]{:S(2)}) copy-start(bf16[2048,512]{1,0:T(8,128)(2,1)} %param.22) | copy-start | bytes 6291460
  20.5 6.6 %copy-start.9 = (bf16[256,512]{1,0:T(8,128)(2,1)S(1)}, bf16[256,512]{1,0:T(8,128)(2,1)}, u32[]{:S(2)}) copy-start(bf16[256,512]{1,0:T(8,128)(2,1)} %param.17) | copy-start | bytes 786436
  20.5 72.7 %all-to-all-start = ((bf16[8,64,2048]{2,1,0:T(8,128)(2,1)}), bf16[8,64,2048]{2,1,0:T(8,128)(2,1)}, u32[]{:S(2)}, u32[]{:S(2)}) async-start(bf16[8,64,2048]{2,1,0:T(8,128)(2,1)} %bitcast.113), calls=%async_computation | async-start | bytes 4194304 | tf_op jit(solution)/shard_map/all_to_all | solution.py:147
  26.9 79.1 %all-gather.7.cloned.1.call-start = ((), (), s32[]{:S(2)}) async-start(), calls=%async_computation.3 | async-start | bytes 2359296 | tf_op jit(solution)/shard_map/all_gather | solution.py:27
  28.6 5.2 %copy-start.10 = (f32[256,4]{0,1:T(4,128)S(1)}, f32[256,4]{0,1:T(4,128)}, u32[]{:S(2)}) copy-start(f32[256,4]{0,1:T(4,128)} %param.21) | copy-start | bytes 12292
  39.4 0.7 copy-start.3
  41.8 2.6 %copy-start.13 = (u32[32]{0:T(128)S(1)}, u32[32]{0:T(128)}, u32[]{:S(2)}) copy-start(u32[32]{0:T(128)} %constant.140) | copy-start | bytes 388
  41.8 40.0 %copy-start.8 = (bf16[256,4,64]{0,2,1:T(8,128)(2,1)S(1)}, bf16[256,4,64]{0,2,1:T(8,128)(2,1)}, u32[]{:S(2)}) copy-start(bf16[256,4,64]{0,2,1:T(8,128)(2,1)} %get-tuple-element.183) | copy-start | bytes 393220
  41.8 40.2 %copy-start.7 = (bf16[256,4,64]{0,2,1:T(8,128)(2,1)S(1)}, bf16[256,4,64]{0,2,1:T(8,128)(2,1)}, u32[]{:S(2)}) copy-start(bf16[256,4,64]{0,2,1:T(8,128)(2,1)} %get-tuple-element.184) | copy-start | bytes 393220
  41.9 40.5 %copy-start.6 = (f32[2,128,4]{2,1,0:T(8,128)S(1)}, f32[2,128,4]{2,1,0:T(8,128)}, u32[]{:S(2)}) copy-start(f32[2,128,4]{2,1,0:T(8,128)} %get-tuple-element.191) | copy-start | bytes 12292
  43.6 0.7 copy-start.1
  44.3 150.6 %all-gather.5.cloned.1.call-start = ((), (), s32[]{:S(2)}) async-start(), calls=%async_computation.2 | async-start | bytes 1310720 | tf_op jit(solution)/shard_map/all_gather | solution.py:117
  93.1 5.3 %copy-start.12 = (bf16[1,2048,1024]{2,1,0:T(8,128)(2,1)S(1)}, bf16[1,2048,1024]{2,1,0:T(8,128)(2,1)}, u32[]{:S(2)}) copy-start(bf16[1,2048,1024]{2,1,0:T(8,128)(2,1)} %param.28) | copy-start | bytes 12582916
  103.5 52.1 %collective-permute-start = (bf16[8,64,1024]{2,1,0:T(8,128)(2,1)}, bf16[8,64,1024]{2,1,0:T(8,128)(2,1)}, u32[]{:S(2)}, u32[]{:S(2)}) collective-permute-start(bf16[8,64,1024]{2,1,0:T(8,128)(2,1)} %multiply_convert_fusion), channel_id=1, source_target_pairs={{0,3},{1,0},{2,1},{3,2},{4,7},{5,4},{6,5},{7,6},{8,11},{9,8},{10,9... | collective-permute-start | bytes 3145736 | tf_op jit(solution)/shard_map/ppermute | solution.py:19
  106.0 43.7 %collective-permute-start.1 = (bf16[8,64,1024]{2,1,0:T(8,128)(2,1)}, bf16[8,64,1024]{2,1,0:T(8,128)(2,1)}, u32[]{:S(2)}, u32[]{:S(2)}) collective-permute-start(bf16[8,64,1024]{2,1,0:T(8,128)(2,1)} %multiply_convert_fusion), channel_id=1, source_target_pairs={{0,1},{1,2},{2,3},{3,0},{4,5},{5,6},{6,7},{7,4},{8,9},{9,10},{10,1... | collective-permute-start | bytes 3145736 | tf_op jit(solution)/shard_map/ppermute | solution.py:17
  106.0 14.9 %copy-start.4 = (bf16[2,128,4,128]{3,1,2,0:T(8,128)(2,1)S(1)}, bf16[2,128,4,128]{3,1,2,0:T(8,128)(2,1)}, u32[]{:S(2)}) copy-start(bf16[2,128,4,128]{3,1,2,0:T(8,128)(2,1)} %copy-done.3) | copy-start | bytes 786436
  106.0 14.9 %copy-start.5 = (bf16[2,128,4,128]{3,2,1,0:T(4,128)(2,1)S(1)}, bf16[2,128,4,128]{3,2,1,0:T(4,128)(2,1)}, u32[]{:S(2)}) copy-start(bf16[2,128,4,128]{3,2,1,0:T(4,128)(2,1)} %reshape.222) | copy-start | bytes 786436
  149.7 27.6 %collective-permute-start.2 = (bf16[8,64,1024]{2,1,0:T(8,128)(2,1)}, bf16[8,64,1024]{2,1,0:T(8,128)(2,1)}, u32[]{:S(2)}, u32[]{:S(2)}) collective-permute-start(bf16[8,64,1024]{2,1,0:T(8,128)(2,1)} %collective-permute-done.1), channel_id=1, source_target_pairs={{0,1},{1,2},{2,3},{3,0},{4,5},{5,6},{6,7},{7,4},{8,9},{9,10},{10,1... | collective-permute-start | bytes 3145736 | tf_op jit(solution)/shard_map/ppermute | solution.py:17
  155.6 2.8 %copy-start.2 = (bf16[1,4096,512]{2,1,0:T(8,128)(2,1)S(1)}, bf16[1,4096,512]{2,1,0:T(8,128)(2,1)}, u32[]{:S(2)}) copy-start(bf16[1,4096,512]{2,1,0:T(8,128)(2,1)} %param.29) | copy-start | bytes 12582916
  160.4 34.3 %copy-start.11 = (f32[256,2]{0,1:T(2,128)S(1)}, f32[256,2]{0,1:T(2,128)}, u32[]{:S(2)}) copy-start(f32[256,2]{0,1:T(2,128)} %param.26) | copy-start | bytes 6148
  180.0 30.1 %all-to-all-start.1 = ((bf16[8,64,512]{2,1,0:T(8,128)(2,1)}), bf16[8,64,512]{2,1,0:T(8,128)(2,1)S(1)}, u32[]{:S(2)}, u32[]{:S(2)}) async-start(bf16[8,64,512]{2,1,0:T(8,128)(2,1)} %fusion.12), calls=%async_computation.1 | async-start | bytes 1048576 | tf_op jit(solution)/shard_map/all_to_all | solution.py:162
Sparse Core Ops, SparseCore 0:
  44.4 48.2 all-gather.6
  153.5 35.6 all-gather.4
